TPU v7x, 32 devices: a whole 2x2x4 slice. The times are simulated.
32 devices in a mesh: ep: 16 (over z, y, x), tp: 2 (over core).
Axes of the slice: x: 2, y: 2, z: 4, core: 2. Of those that a mesh axis runs over, the one named last changes fastest.
Arguments:
- hidden: bfloat16 [1024, 2048], P('ep'), may hold values from -6 to 6
- mix_gain: float32 [2048], replicated, may hold values from 0.1 to 1.9
- recept_weight: bfloat16 [2048, 1024], P(None, 'tp'), may hold values from -0.125 to 0.125
- key_weight: bfloat16 [2048, 1024], P(None, 'tp'), may hold values from -0.125 to 0.125
- value_weight: bfloat16 [2048, 1024], P(None, 'tp'), may hold values from -0.125 to 0.125
- decay_down: bfloat16 [2048, 64], replicated, may hold values from -0.125 to 0.125
- decay_up: bfloat16 [64, 1024], replicated, may hold values from -0.75 to 0.75
- decay_bias: float32 [1024], replicated, may hold values from -4 to 1
- rate_down: bfloat16 [2048, 64], replicated, may hold values from -0.125 to 0.125
- rate_up: bfloat16 [64, 1024], replicated, may hold values from -0.75 to 0.75
- rate_bias: float32 [1024], replicated, may hold values from -4 to 4
- head_gain: float32 [1024], replicated, may hold values from 0.1 to 1.9
- out_weight: bfloat16 [1024, 2048], P('tp'), may hold values from -0.1875 to 0.1875
- memory_state: float32 [1024, 16, 64, 64], P('ep', 'tp'), may hold values from -6 to 6
- ffn_gain: float32 [2048], replicated, may hold values from 0.1 to 1.9
- blend_vector: bfloat16 [2048], replicated, may hold values from -0.125 to 0.125
- dense_gate: bfloat16 [2048, 5632], P(None, ('ep', 'tp')), may hold values from -0.125 to 0.125
- dense_up: bfloat16 [2048, 5632], P(None, ('ep', 'tp')), may hold values from -0.125 to 0.125
- dense_down: bfloat16 [5632, 2048], P(('ep', 'tp')), may hold values from -0.3125 to 0.3125
- expert_gate: bfloat16 [16, 2048, 1536], P('ep', None, 'tp'), may hold values from -0.125 to 0.125
- expert_up: bfloat16 [16, 2048, 1536], P('ep', None, 'tp'), may hold values from -0.125 to 0.125
- expert_down: bfloat16 [16, 1536, 2048], P('ep', 'tp'), may hold values from -0.15625 to 0.15625
- routing: int32 [1024, 2], P('ep'), may hold values from 0 to 15, all different within a row; in each aligned block of 64 rows (0 to 63, 64 to 127, ...) at most 16 rows name the same one
- route_scale: float32 [1024, 2], P('ep'), may hold values from 0.25 to 1
Outputs:
- layer_out: bfloat16 [1024, 2048], P('ep')
- new_state: float32 [1024, 16, 64, 64], P('ep', 'tp')
Inputs may be any that keep to these rules, and one draw needn't show every extreme that they name: `routing`: among the 64 sequences of one index of ep, no expert is chosen more than 16 times, and some expert is chosen exactly 16 times; a sequence's 2 choices differ.
All inputs are finite; a program needn't handle non-finite values.
Results may differ from a plain program's by a relative error of at most 0.017.
Values may be sent and summed in bfloat16 or wider, within the bound.
A program may use at most 192 MiB of HBM per device.

v0:
```python
import jax
import jax.numpy as jnp
from jax import lax
from jax.sharding import PartitionSpec as P


def stored(tensor):
    return lax.optimization_barrier(tensor.astype(jnp.bfloat16)).astype(jnp.float32)


def rms_scaled(tensor, gain_vec):
    values = tensor.astype(jnp.float32)
    return values * lax.rsqrt(jnp.mean(values * values, axis=-1, keepdims=True) + 1e-06) * gain_vec


def silu_of(tensor):
    return tensor / (1.0 + jnp.exp(-tensor))


def matmul(left, right):
    return jnp.dot(left, right, preferred_element_type=jnp.float32)


def shards(
    hidden,
    mix_gain,
    recept_weight,
    key_weight,
    value_weight,
    decay_down,
    decay_up,
    decay_bias,
    rate_down,
    rate_up,
    rate_bias,
    head_gain,
    out_weight,
    memory_state,
    ffn_gain,
    blend_vector,
    dense_gate,
    dense_up,
    dense_down,
    expert_gate,
    expert_up,
    expert_down,
    routing,
    route_scale,
):
    seq_count, model_width = hidden.shape
    own_width = recept_weight.shape[1]
    head_count = memory_state.shape[1]
    head_size = memory_state.shape[2]
    offset = lax.axis_index("tp") * own_width
    decay_up_own = lax.dynamic_slice_in_dim(decay_up, offset, own_width, 1)
    rate_up_own = lax.dynamic_slice_in_dim(rate_up, offset, own_width, 1)
    decay_bias_own = lax.dynamic_slice_in_dim(decay_bias, offset, own_width, 0)
    rate_bias_own = lax.dynamic_slice_in_dim(rate_bias, offset, own_width, 0)
    gain_own = lax.dynamic_slice_in_dim(head_gain, offset, own_width, 0)
    normed_in = rms_scaled(hidden, mix_gain).astype(jnp.bfloat16)
    split_shape = (seq_count, head_count, head_size)
    recept_rows = stored(matmul(normed_in, recept_weight)).reshape(split_shape)
    key_rows = stored(matmul(normed_in, key_weight)).reshape(split_shape)
    value_rows = stored(matmul(normed_in, value_weight)).reshape(split_shape)
    decay_low = jnp.tanh(matmul(normed_in, decay_down)).astype(jnp.bfloat16)
    decay_pre = matmul(decay_low, decay_up_own) + decay_bias_own
    decay_rate = jnp.exp(-jnp.exp(-jax.nn.softplus(-decay_pre) - 0.5)).reshape(split_shape)
    rate_low = matmul(normed_in, rate_down).astype(jnp.bfloat16)
    learn_rate = jax.nn.sigmoid(matmul(rate_low, rate_up_own) + rate_bias_own).reshape(split_shape)
    unit_key = key_rows * lax.rsqrt(jnp.sum(key_rows * key_rows, axis=-1, keepdims=True) + 1e-06)
    removed = jnp.einsum("shij,shj->shi", memory_state, unit_key, precision=lax.Precision.HIGHEST)
    new_state = (
        memory_state * decay_rate[:, :, None, :]
        - removed[..., None] * (unit_key * learn_rate)[:, :, None, :]
        + value_rows[..., None] * (key_rows * learn_rate)[:, :, None, :]
    )
    readout = jnp.einsum("shij,shj->shi", new_state, recept_rows, precision=lax.Precision.HIGHEST)
    centre = jnp.mean(readout, axis=-1, keepdims=True)
    variance = jnp.mean(jnp.square(readout - centre), axis=-1, keepdims=True)
    head_normed = (
        (
            (readout - centre)
            * lax.rsqrt(variance + 0.00064)
            * gain_own.reshape(head_count, head_size)
        )
        .astype(jnp.bfloat16)
        .reshape(seq_count, own_width)
    )
    attn_sum = lax.psum(matmul(head_normed, out_weight).astype(jnp.bfloat16), "tp").astype(
        jnp.float32
    )
    first_res = (hidden.astype(jnp.float32) + attn_sum).astype(jnp.bfloat16)
    ffn_in = rms_scaled(first_res, ffn_gain).astype(jnp.bfloat16)
    blend = jax.nn.sigmoid(jnp.dot(ffn_in, blend_vector, preferred_element_type=jnp.float32))
    piece = lax.all_gather(ffn_in, "ep", axis=0, tiled=True)
    dense_act = (silu_of(matmul(piece, dense_gate)) * matmul(piece, dense_up)).astype(jnp.bfloat16)
    own_units = lax.all_to_all(dense_act, "ep", split_axis=0, concat_axis=1, tiled=True)
    dense_out = matmul(own_units, lax.all_gather(dense_down, "ep", axis=0, tiled=True))
    dest_count = lax.axis_size("ep")
    top_count = routing.shape[1]
    slot_cap = max(2, 2 * seq_count * top_count // dest_count)
    flat_route = routing.reshape(-1)
    one_hot = (flat_route[:, None] == jnp.arange(dest_count, dtype=jnp.int32)[None, :]).astype(
        jnp.int32
    )
    running = jnp.cumsum(one_hot, axis=0)
    rank = jnp.sum((running - 1) * one_hot, axis=1)
    slot = flat_route * slot_cap + rank
    select = (slot[None, :] == jnp.arange(dest_count * slot_cap, dtype=jnp.int32)[:, None]).astype(
        jnp.bfloat16
    )
    pair_rows = jnp.repeat(ffn_in, top_count, axis=0)
    outgoing = (
        matmul(select, pair_rows).astype(jnp.bfloat16).reshape(dest_count, slot_cap, model_width)
    )
    arrived = lax.all_to_all(outgoing, "ep", split_axis=0, concat_axis=0, tiled=True)
    src_count, slot_items, width_in = arrived.shape
    flat_in = arrived.reshape(src_count * slot_items, width_in)
    expert_act = (silu_of(matmul(flat_in, expert_gate[0])) * matmul(flat_in, expert_up[0])).astype(
        jnp.bfloat16
    )
    result = matmul(expert_act, expert_down[0]).reshape(src_count, slot_items, width_in)
    returned = lax.all_to_all(
        result.astype(jnp.bfloat16), "ep", split_axis=0, concat_axis=0, tiled=True
    ).astype(result.dtype)
    per_pair = jnp.take(returned.reshape(dest_count * slot_cap, model_width), slot, axis=0)
    expert_sum = jnp.sum(
        per_pair.reshape(seq_count, top_count, model_width) * route_scale[:, :, None], axis=1
    )
    mixed = lax.psum((expert_sum + blend[:, None] * dense_out).astype(jnp.bfloat16), "tp").astype(
        jnp.float32
    )
    layer_out = (first_res.astype(jnp.float32) + mixed).astype(jnp.bfloat16)
    return (layer_out, new_state)


def solution(mesh):
    in_specs = (
        P("ep", None),
        P(),
        P(None, "tp"),
        P(None, "tp"),
        P(None, "tp"),
        P(),
        P(),
        P(),
        P(),
        P(),
        P(),
        P(),
        P("tp", None),
        P("ep", "tp", None, None),
        P(),
        P(),
        P(None, ("ep", "tp")),
        P(None, ("ep", "tp")),
        P(("ep", "tp"), None),
        P("ep", None, "tp"),
        P("ep", None, "tp"),
        P("ep", "tp", None),
        P("ep", None),
        P("ep", None),
    )
    out_specs = (P("ep", None), P("ep", "tp", None, None))
    return jax.shard_map(shards, mesh=mesh, in_specs=in_specs, out_specs=out_specs, check_vma=False)
```

profile of v0, /device:TPU:0, one launch (start us, length us, event | category | flops | bytes accessed | tf_op | source)
XLA Modules:
  0.0 408.8 jit_solution(1007329135840309137)
XLA Ops:
  9.3 1.5 fusion.21
  11.6 2.2 convolution_convert_fusion.4
  19.4 2.1 convolution_convert_fusion.3
  22.3 2.1 convolution_convert_fusion.2
  26.7 29.5 %fusion.56 = f32[64,8,1,64]{3,2,1,0:T(1,128)S(1)} fusion(f32[64,8,64,1]{2,3,1,0:T(1,128)S(1)} %bitcast.78, f32[64,8,64,64]{3,2,1,0:T(8,128)} %param.37), kind=kOutput, calls=%fused_computation.85 | convolution fusion | flops 25165824 | bytes 8650752 | tf_op jit(solution)/shard_map/shij,shj->shi/dot_general | solution.py:71
  56.3 11.9 %multiply_add_fusion = f32[64,8,64,64]{3,2,1,0:T(8,128)} fusion(f32[64,8,64,64]{3,2,1,0:T(8,128)S(1)} %bitcast.71, f32[64,8,64]{2,1,0:T(8,128)S(1)} %get-tuple-element.4, f32[64,8,64]{2,1,0:T(8,128)S(1)} %copy-done.3, f32[64,8,64]{2,1,0:T(8,128)S(1)} %get-tuple-element.2, f32[64,8,64]{2,1,0:T(8,128)S(1)} %bitcast.77, f32[64,8,64]{2,1,0:T(8,128)S(1)} %copy-done.4), kind=kLoop, calls=%fused_computation.1 | loop fusion | flops 10485760 | bytes 17432576 | tf_op jit(solution)/shard_map/add | solution.py:73
  68.2 16.3 %fusion.57 = f32[64,8,1,64]{3,2,1,0:T(1,128)} fusion(f32[64,8,64,64]{3,2,1,0:T(8,128)} %multiply_add_fusion, bf16[64,8,64,1]{2,3,1,0:T(2,128)(2,1)S(1)} %copy-done.2), kind=kOutput, calls=%fused_computation.86 | convolution fusion | flops 25165824 | bytes 8585216 | tf_op jit(solution)/shard_map/shij,shj->shi/dot_general | solution.py:77
  90.2 2.8 convolution_convert_fusion.1
  93.3 20.9 %all-reduce.3.cloned.1.call-done = bf16[64,2048]{1,0:T(8,128)(2,1)} async-done(((bf16[64,2048]{1,0:T(8,128)(2,1)}), bf16[64,2048]{1,0:T(8,128)(2,1)}) %all-reduce.3.cloned.1.call-update) | async-done | bytes 262160 | tf_op jit(solution)/shard_map/psum | solution.py:89
  115.3 1.8 fusion.34
  118.5 2.1 broadcast_in_dim.10
  120.6 2.1 reshape.162
  122.7 1.6 convolution_convert_fusion
  124.3 45.4 %all_to_all.29 = bf16[16,16,2048]{2,1,0:T(8,128)(2,1)S(1)} all-to-all(bf16[16,16,2048]{2,1,0:T(8,128)(2,1)S(1)} %bitcast.75), channel_id=1, replica_groups=mesh['ep'=16,'tp'=2] {'ep'}, dimensions={0} | all-to-all | bytes 2097152 | tf_op jit(solution)/shard_map/all_to_all | solution.py:116
  172.6 2.0 fusion.6
  174.6 6.8 %all-to-all-start.1 = ((bf16[16,16,2048]{2,1,0:T(8,128)(2,1)}), bf16[16,16,2048]{2,1,0:T(8,128)(2,1)}, u32[]{:S(2)}, u32[]{:S(2)}) async-start(bf16[16,16,2048]{2,1,0:T(8,128)(2,1)} %fusion.6), calls=%async_computation.1 | async-start | bytes 2097152 | tf_op jit(solution)/shard_map/all_to_all | solution.py:123
  183.3 38.9 %all-gather.3.cloned.1.call-done = bf16[1024,2048]{1,0:T(8,128)(2,1)} async-done(((bf16[64,2048]{1,0:T(8,128)(2,1)}), bf16[1024,2048]{1,0:T(8,128)(2,1)}) %all-gather.3.cloned.1.call-update) | async-done | bytes 4194320 | tf_op jit(solution)/shard_map/all_gather | solution.py:95
  222.2 4.1 fusion.58
  226.3 2.3 fusion.17
  228.6 2.0 copy.44
  230.6 4.7 %all-to-all-start.2 = ((bf16[16,64,176]{2,1,0:T(8,128)(2,1)}), bf16[16,64,176]{2,1,0:T(8,128)(2,1)}, u32[]{:S(2)}, u32[]{:S(2)}) async-start(bf16[16,64,176]{2,1,0:T(8,128)(2,1)} %bitcast.76), calls=%async_computation.2 | async-start | bytes 1048576 | tf_op jit(solution)/shard_map/all_to_all | solution.py:97
  235.6 2.9 bitcast_convert_fusion
  238.5 4.0 gather_fusion
  242.5 2.8 gather.7
  245.3 4.2 %multiply_reduce_fusion = f32[64,2048]{1,0:T(8,128)} fusion(f32[64,2,2048]{2,1,0:T(2,128)} %gather.7, pred[64,2]{1,0:T(8,128)(4,1)S(1)} %copy.41, f32[64,2]{1,0:T(8,128)S(1)} %copy.43), kind=kLoop, calls=%fused_computation.37 | loop fusion | flops 655360 | bytes 1573504 | tf_op jit(solution)/shard_map/reduce_sum | solution.py:127
  249.5 8.7 %all-to-all-done.2 = bf16[16,64,176]{2,1,0:T(8,128)(2,1)} async-done(((bf16[16,64,176]{2,1,0:T(8,128)(2,1)}), bf16[16,64,176]{2,1,0:T(8,128)(2,1)}, u32[]{:S(2)}, u32[]{:S(2)}) %all-to-all-start.2) | async-done | bytes 360480 | tf_op jit(solution)/shard_map/all_to_all | solution.py:97
  258.2 2.1 copy.45
  260.3 2.5 all_to_all.25
  262.8 113.8 %all-gather.5.cloned.1.call-done = bf16[2816,2048]{1,0:T(8,128)(2,1)} async-done(((bf16[176,2048]{1,0:T(8,128)(2,1)}), bf16[2816,2048]{1,0:T(8,128)(2,1)}) %all-gather.5.cloned.1.call-update) | async-done | bytes 11534352 | tf_op jit(solution)/shard_map/all_gather | solution.py:98
  376.6 7.2 %fusion.10 = bf16[64,2048]{1,0:T(8,128)(2,1)} fusion(f32[64,2048]{1,0:T(8,128)} %multiply_reduce_fusion, bf16[64,2816]{1,0:T(8,128)(2,1)} %all_to_all.25, bf16[2816,2048]{1,0:T(8,128)(2,1)} %all-gather.5.cloned.1.call-done, f32[64]{0:T(128)S(1)} %fusion.27), kind=kOutput, calls=%fused_computation.13 | convolution fusion | flops 738590720 | bytes 12681472 | tf_op jit(solution)/shard_map/dot_general | solution.py:21
  383.9 16.6 %all-reduce.5.cloned.1.call-done = bf16[64,2048]{1,0:T(8,128)(2,1)} async-done(((bf16[64,2048]{1,0:T(8,128)(2,1)}), bf16[64,2048]{1,0:T(8,128)(2,1)}) %all-reduce.5.cloned.1.call-update) | async-done | bytes 262160 | tf_op jit(solution)/shard_map/psum | solution.py:130
  400.4 1.8 fusion.35
  (95 shorter events, 24.9 us)
Async XLA Ops:
  7.2 165.4 %copy-start = (bf16[1,768,2048]{2,1,0:T(8,128)(2,1)S(1)}, bf16[1,768,2048]{2,1,0:T(8,128)(2,1)}, u32[]{:S(2)}) copy-start(bf16[1,768,2048]{2,1,0:T(8,128)(2,1)} %param.45) | copy-start | bytes 9437188
  7.2 9.9 %copy-start.1 = (bf16[64,2048]{1,0:T(8,128)(2,1)S(1)}, bf16[64,2048]{1,0:T(8,128)(2,1)}, u32[]{:S(2)}) copy-start(bf16[64,2048]{1,0:T(8,128)(2,1)} %param.24) | copy-start | bytes 786436
  7.2 9.9 %copy-start.7 = (f32[2048]{0:T(1024)S(1)}, f32[2048]{0:T(1024)}, u32[]{:S(2)}) copy-start(f32[2048]{0:T(1024)} %param.25) | copy-start | bytes 24580
  7.2 106.9 %all-reduce.3.cloned.1.call-start = ((), (), s32[]{:S(2)}) async-start(), calls=%async_computation.3 | async-start | bytes 524288 | tf_op jit(solution)/shard_map/psum | solution.py:89
  19.4 5.9 %copy-start.6 = (f32[64,8]{1,0:T(8,128)S(1)}, f32[64,8]{1,0:T(8,128)}, u32[]{:S(2)}) copy-start(f32[64,8]{1,0:T(8,128)} %add_rsqrt_fusion.1) | copy-start | bytes 6148
  25.3 30.9 %slice-start = ((s8[16777216]{0:T(1024)(128)(4,1)}), s8[4194304]{0:T(1024)(128)(4,1)S(1)}, s32[]{:S(2)}) async-start(s8[16777216]{0:T(1024)(128)(4,1)} %bitcast.70), calls=%async_computation.7 | async-start | bytes 8388608
  26.7 29.6 %slice-start.1 = ((s8[16777216]{0:T(1024)(128)(4,1)}), s8[4194304]{0:T(1024)(128)(4,1)S(1)}, s32[]{:S(2)}) async-start(s8[16777216]{0:T(1024)(128)(4,1)} %bitcast.70), calls=%async_computation.8 | async-start | bytes 8388608
  26.7 29.6 %slice-start.2 = ((s8[16777216]{0:T(1024)(128)(4,1)}), s8[4194304]{0:T(1024)(128)(4,1)S(1)}, s32[]{:S(2)}) async-start(s8[16777216]{0:T(1024)(128)(4,1)} %bitcast.70), calls=%async_computation.9 | async-start | bytes 8388608
  26.7 29.6 %slice-start.3 = ((s8[16777216]{0:T(1024)(128)(4,1)}), s8[4194304]{0:T(1024)(128)(4,1)S(1)}, s32[]{:S(2)}) async-start(s8[16777216]{0:T(1024)(128)(4,1)} %bitcast.70), calls=%async_computation.10 | async-start | bytes 8388608
  26.7 29.6 %copy-start.3 = (f32[64,8,64]{2,1,0:T(8,128)S(1)}, f32[64,8,64]{2,1,0:T(8,128)}, u32[]{:S(2)}) copy-start(f32[64,8,64]{2,1,0:T(8,128)} %reshape.169) | copy-start | bytes 393220
  26.7 29.6 %copy-start.4 = (f32[64,8,64]{2,1,0:T(8,128)S(1)}, f32[64,8,64]{2,1,0:T(8,128)}, u32[]{:S(2)}) copy-start(f32[64,8,64]{2,1,0:T(8,128)} %mul.187) | copy-start | bytes 393220
  56.3 11.9 %copy-start.2 = (bf16[64,8,64,1]{2,3,1,0:T(2,128)(2,1)S(1)}, bf16[64,8,64,1]{2,3,1,0:T(2,128)(2,1)}, u32[]{:S(2)}) copy-start(bf16[64,8,64,1]{2,3,1,0:T(2,128)(2,1)} %reshape.188) | copy-start | bytes 196612
  68.2 19.9 %copy-start.12 = (f32[1024]{0:T(1024)S(1)}, f32[1024]{0:T(1024)}, u32[]{:S(2)}) copy-start(f32[1024]{0:T(1024)} %param.35) | copy-start | bytes 12292
  84.5 30.8 %copy-start.9 = (f32[2048]{0:T(1024)S(1)}, f32[2048]{0:T(1024)}, u32[]{:S(2)}) copy-start(f32[2048]{0:T(1024)} %param.38) | copy-start | bytes 24580
  84.5 33.3 %copy-start.8 = (s32[64,2]{0,1:T(2,128)S(1)}, s32[64,2]{0,1:T(2,128)}, u32[]{:S(2)}) copy-start(s32[64,2]{0,1:T(2,128)} %param.46) | copy-start | bytes 1540
  85.7 0.6 copy-start.5
  93.0 129.2 %all-gather.3.cloned.1.call-start = ((), (), s32[]{:S(2)}) async-start(), calls=%async_computation.4 | async-start | bytes 4456448 | tf_op jit(solution)/shard_map/all_gather | solution.py:95
  117.1 259.5 %all-gather.5.cloned.1.call-start = ((), (), s32[]{:S(2)}) async-start(), calls=%async_computation.5 | async-start | bytes 12255232 | tf_op jit(solution)/shard_map/all_gather | solution.py:98
  122.7 47.0 %copy-start.14 = (bf16[1,2048,768]{2,1,0:T(8,128)(2,1)S(1)}, bf16[1,2048,768]{2,1,0:T(8,128)(2,1)}, u32[]{:S(2)}) copy-start(bf16[1,2048,768]{2,1,0:T(8,128)(2,1)} %param.43) | copy-start | bytes 9437188
  169.7 1.9 copy-start.15
  172.6 9.4 %copy-start.11 = (f32[64,2]{0,1:T(2,128)S(1)}, f32[64,2]{0,1:T(2,128)}, u32[]{:S(2)}) copy-start(f32[64,2]{0,1:T(2,128)} %param.47) | copy-start | bytes 1540
  172.6 9.5 %copy-start.10 = (bf16[2048]{0:T(1024)(128)(2,1)S(1)}, bf16[2048]{0:T(1024)(128)(2,1)}, u32[]{:S(2)}) copy-start(bf16[2048]{0:T(1024)(128)(2,1)} %param.39) | copy-start | bytes 12292
  174.6 56.0 %all-to-all-start.1 = ((bf16[16,16,2048]{2,1,0:T(8,128)(2,1)}), bf16[16,16,2048]{2,1,0:T(8,128)(2,1)}, u32[]{:S(2)}, u32[]{:S(2)}) async-start(bf16[16,16,2048]{2,1,0:T(8,128)(2,1)} %fusion.6), calls=%async_computation.1 | async-start | bytes 2097152 | tf_op jit(solution)/shard_map/all_to_all | solution.py:123
  222.2 4.1 copy-start.13
  222.2 4.1 copy-start.16
  230.6 27.6 %all-to-all-start.2 = ((bf16[16,64,176]{2,1,0:T(8,128)(2,1)}), bf16[16,64,176]{2,1,0:T(8,128)(2,1)}, u32[]{:S(2)}, u32[]{:S(2)}) async-start(bf16[16,64,176]{2,1,0:T(8,128)(2,1)} %bitcast.76), calls=%async_computation.2 | async-start | bytes 1048576 | tf_op jit(solution)/shard_map/all_to_all | solution.py:97
  235.3 165.1 %all-reduce.5.cloned.1.call-start = ((), (), s32[]{:S(2)}) async-start(), calls=%async_computation.6 | async-start | bytes 524288 | tf_op jit(solution)/shard_map/psum | solution.py:130
Sparse Core Ops, SparseCore 0:
  93.1 20.9 all-reduce.2
  117.5 104.6 all-gather.2
  224.9 151.6 all-gather.4
  384.0 16.3 all-reduce.4
where the time goes:
time: 410 us; the launch traced here: 409 us
  waiting for transfers between devices  200 us (49%)
  matrix products  78.4 us (19%)
  blocking collectives  45.4 us (11%)
  other arithmetic  32.6 us (8%)
  local copies, waits for them, and re-layouts  26.6 us (6%)
  between operations  14.2 us (3%)
  starting transfers between devices  12.1 us (3%)
    all_gather x1, waiting for transfers between devices, shards(): lax.all_gather(dense_down, 'ep', axis=0, tiled=True)  114 us
    all_to_all x1, blocking collectives, shards(): lax.all_to_all(outgoing, 'ep', split_axis=0, concat_axis=0, tiled=True)  45.4 us
    all_gather x1, waiting for transfers between devices, shards(): piece = lax.all_gather(ffn_in, 'ep', axis=0, tiled=True)  38.9 us
    dot_general x13, matrix products, matmul(): return jnp.dot(left, right, preferred_element_type=jnp.float32)  31.5 us
    dot_general x1, matrix products, shards(): jnp.einsum('shij,shj->shi', memory_state, unit_key, precision=lax.Precisi...  29.5 us
    psum x1, waiting for transfers between devices, shards(): lax.psum(matmul(head_normed, out_weight).astype(jnp.bfloat16), 'tp')  20.9 us
    psum x1, waiting for transfers between devices, shards(): lax.psum((expert_sum + blend[:, None] * dense_out).astype(jnp.bfloat16),...  16.6 us
    dot_general x1, matrix products, shards(): jnp.einsum('shij,shj->shi', new_state, recept_rows, precision=lax.Precisi...  16.3 us
  transfers between devices with their start and end apart: 6, of which 5 were waited for; matrix products, arithmetic and copies ran while one was open for 9% of the time, Pallas kernels for 0%

commit v1 on v0

v1 whole, which is shorter than its diff:
```python
import functools
import math

import jax
import jax.numpy as jnp
from jax import lax
from jax.experimental import pallas as pl
from jax.experimental.pallas import tpu as pltpu
from jax.sharding import PartitionSpec as P

MESH = pl.DeviceIdType.MESH
F32 = jnp.float32
BF16 = jnp.bfloat16
VMEM_LIMIT = 64 * 1024 * 1024 - 65536
VMEM_SPEC = pl.BlockSpec(memory_space=pltpu.VMEM)


def matmul(left, right):
    return jnp.dot(left, right, preferred_element_type=F32)


def silu_of(tensor):
    return tensor / (1.0 + jnp.exp(-tensor))


def rms_scaled(values, gain):
    return values * lax.rsqrt(jnp.mean(values * values, axis=-1, keepdims=True) + 1e-06) * gain


def factors_of(count):
    slow = 4 if count % 4 == 0 else 1
    rest = count // slow
    mid = math.isqrt(rest)
    while rest % mid:
        mid -= 1
    return slow, mid, rest // mid


def attention_kernel(
    step_rows,
    hidden,
    mix_gain,
    recept_weight,
    key_weight,
    value_weight,
    decay_down,
    decay_up,
    decay_bias,
    rate_down,
    rate_up,
    rate_bias,
    head_gain,
    out_weight,
    state_in,
    state_out,
    partial,
    recept_s,
    unit_s,
    unit_rate_s,
    key_rate_s,
    value_s,
    decay_s,
    readout_s,
    normed_s,
):
    step = pl.program_id(0)
    heads, seqs, size = recept_s.shape
    width = heads * size
    own = pl.ds(pl.multiple_of(lax.axis_index("tp") * width, 128), width)

    @pl.when(step == 0)
    def _():
        normed = rms_scaled(hidden[...].astype(F32), mix_gain[...]).astype(BF16)
        recept = matmul(normed, recept_weight[...]).astype(BF16).astype(F32)
        keys = matmul(normed, key_weight[...]).astype(BF16).astype(F32)
        vals = matmul(normed, value_weight[...]).astype(BF16).astype(F32)
        decay_low = jnp.tanh(matmul(normed, decay_down[...])).astype(BF16)
        decay_pre = matmul(decay_low, decay_up[:, own]) + decay_bias[:, own]
        softplus = jnp.maximum(-decay_pre, 0.0) + jnp.log1p(jnp.exp(-jnp.abs(decay_pre)))
        decay = jnp.exp(-jnp.exp(-softplus - 0.5))
        rate_low = matmul(normed, rate_down[...]).astype(BF16)
        rate = 1.0 / (1.0 + jnp.exp(-(matmul(rate_low, rate_up[:, own]) + rate_bias[:, own])))
        for h in range(heads):
            cols = slice(h * size, (h + 1) * size)
            key_h, rate_h = keys[:, cols], rate[:, cols]
            unit = key_h * lax.rsqrt(jnp.sum(key_h * key_h, axis=-1, keepdims=True) + 1e-06)
            recept_s[h] = recept[:, cols]
            unit_s[h] = unit
            unit_rate_s[h] = unit * rate_h
            key_rate_s[h] = key_h * rate_h
            value_s[h] = vals[:, cols]
            decay_s[h] = decay[:, cols]

    eye = (
        lax.broadcasted_iota(jnp.int32, (size, size), 0)
        == lax.broadcasted_iota(jnp.int32, (size, size), 1)
    ).astype(F32)

    def one_sequence(local, carry):
        row = pl.ds(step * step_rows + local, 1)
        for h in range(heads):
            state = state_in[local, h]
            removed = jnp.sum(state * unit_s[h, row], axis=-1, keepdims=True)
            value = jnp.sum(eye * value_s[h, row], axis=-1, keepdims=True)
            new = (
                state * decay_s[h, row]
                - removed * unit_rate_s[h, row]
                + value * key_rate_s[h, row]
            )
            state_out[local, h] = new
            out = jnp.sum(new * recept_s[h, row], axis=-1, keepdims=True)
            readout_s[h, row] = jnp.sum(eye * out, axis=0, keepdims=True)
        return carry

    lax.fori_loop(0, step_rows, one_sequence, 0)

    @pl.when(step == pl.num_programs(0) - 1)
    def _():
        gain = head_gain[:, own]
        for h in range(heads):
            cols = slice(h * size, (h + 1) * size)
            out = readout_s[h]
            centred = out - jnp.mean(out, axis=-1, keepdims=True)
            variance = jnp.mean(centred * centred, axis=-1, keepdims=True)
            normed_s[:, cols] = (centred * lax.rsqrt(variance + 0.00064) * gain[:, cols]).astype(BF16)
        partial[...] = matmul(normed_s[...], out_weight[...]).astype(BF16)


def attention(hidden, vectors, state):
    seqs, heads, size, _ = state.shape
    width = heads * size
    step_rows = math.gcd(seqs, 8)
    block = pl.BlockSpec((step_rows, heads, size, size), lambda i: (i, 0, 0, 0))
    operands = (hidden,) + vectors
    whole = [pl.BlockSpec(a.shape, lambda i: (0, 0)) for a in operands]
    per_head = pltpu.VMEM((heads, seqs, size), F32)
    return pl.pallas_call(
        functools.partial(attention_kernel, step_rows),
        grid=(seqs // step_rows,),
        out_shape=(
            jax.ShapeDtypeStruct(state.shape, F32),
            jax.ShapeDtypeStruct(hidden.shape, BF16),
        ),
        in_specs=whole + [block],
        out_specs=(block, pl.BlockSpec(hidden.shape, lambda i: (0, 0))),
        scratch_shapes=[per_head] * 7 + [pltpu.VMEM((seqs, width), BF16)],
        compiler_params=pltpu.CompilerParams(
            dimension_semantics=("arbitrary",), vmem_limit_bytes=VMEM_LIMIT
        ),
        name="attention",
    )(*operands, state)


def position(sizes):
    ep = lax.axis_index("ep")
    strides = (sizes[1] * sizes[2], sizes[2], 1)
    return ep, tuple(ep // s % n for s, n in zip(strides, sizes)), strides


def greet_all(count):
    ep, tp = lax.axis_index("ep"), lax.axis_index("tp")
    barrier = pltpu.get_barrier_semaphore()

    def greet(k, carry):
        pl.semaphore_signal(
            barrier, inc=1, device_id=((ep + k) % count, tp), device_id_type=MESH
        )
        return carry

    lax.fori_loop(1, count, greet, 0)
    pl.semaphore_signal(barrier, inc=1, device_id=(ep, 1 - tp), device_id_type=MESH)
    pl.semaphore_wait(barrier, count)


def remote(src, dst, send, recv, device):
    return pltpu.make_async_remote_copy(
        src_ref=src,
        dst_ref=dst,
        send_sem=send,
        recv_sem=recv,
        device_id=device,
        device_id_type=MESH,
    )


def gather_kernel(
    sizes,
    partial,
    hidden,
    gain,
    meta,
    first,
    tokens,
    metas,
    sibling_part,
    part_sem,
    meta_send,
    meta_recv,
    own_sem,
    send_sem,
    recv_sem,
    pass_send,
    pass_recv,
):
    count = sizes[0] * sizes[1] * sizes[2]
    ep, at, strides = position(sizes)
    tp = lax.axis_index("tp")
    half = first.shape[0]
    mine = pl.ds(pl.multiple_of(tp * half, half), half)
    other = pl.ds(pl.multiple_of((1 - tp) * half, half), half)
    greet_all(count)
    swap = remote(partial.at[other], sibling_part, part_sem.at[0], part_sem.at[1], (ep, 1 - tp))
    swap.start()

    def meta_copy(k):
        return remote(
            meta, metas.at[ep], meta_send.at[k], meta_recv.at[k], ((ep + k) % count, tp)
        )

    def start_meta(k, carry):
        meta_copy(k).start()
        return carry

    lax.fori_loop(1, count, start_meta, 0)
    metas[ep] = meta[...]
    swap.wait()
    total = (
        hidden[mine, :].astype(F32)
        + partial[mine, :].astype(F32)
        + sibling_part[...].astype(F32)
    ).astype(BF16)
    first[...] = total
    ffn_in = rms_scaled(total.astype(F32), gain[...]).astype(BF16)
    tokens[at[0], at[1], at[2], mine, :] = ffn_in

    def blocks(order):
        held = [pl.ds(c, 1) for c in at]
        for d in order:
            before = tuple(held)
            for k in range(1, sizes[d]):
                come = list(held)
                come[d] = pl.ds((at[d] + sizes[d] - k) % sizes[d], 1)
                yield d, k, before, tuple(come)
            held[d] = pl.ds(0, sizes[d])

    def run(core, order, order_of_other):
        rows = pl.ds(core * half, half)
        rows_of_other = pl.ds((1 - core) * half, half)
        sibling = (ep, 1 - core)

        def own_copy(r):
            view = tokens.at[pl.ds(at[0], 1), pl.ds(at[1], 1), pl.ds(at[2], 1), r]
            return remote(view, view, own_sem.at[0], own_sem.at[1], sibling)

        def pass_copy(d, k, come, r):
            view = tokens.at[come + (r,)]
            return remote(view, view, pass_send.at[d, k], pass_recv.at[d, k], sibling)

        to_wait = [own_copy(rows)]
        to_wait[0].start()
        steps = list(blocks(order))
        for d in order:
            copies = []
            for dd, k, before, come in steps:
                if dd == d:
                    peer = ep + ((at[d] + k) % sizes[d] - at[d]) * strides[d]
                    view = tokens.at[before + (rows,)]
                    copy = remote(view, view, send_sem.at[d, k], recv_sem.at[d, k], (peer, core))
                    copy.start()
                    copies.append((copy, k, come))
            for copy, k, come in copies:
                copy.wait()
                onward = pass_copy(d, k, come, rows)
                onward.start()
                to_wait.append(onward)
        for copy in to_wait:
            copy.wait_send()
        own_copy(rows_of_other).wait_recv()
        for d, k, before, come in blocks(order_of_other):
            pass_copy(d, k, come, rows_of_other).wait_recv()

    @pl.when(tp == 0)
    def _():
        run(0, (2, 1, 0), (0, 1, 2))

    @pl.when(tp == 1)
    def _():
        run(1, (0, 1, 2), (2, 1, 0))

    def wait_meta(k, carry):
        meta_copy(k).wait()
        return carry

    lax.fori_loop(1, count, wait_meta, 0)


def gather_tokens(sizes, partial, hidden, gain, meta):
    seqs, width = hidden.shape
    count = sizes[0] * sizes[1] * sizes[2]
    half = seqs // 2
    most = max(sizes)
    dma = pltpu.SemaphoreType.DMA
    return pl.pallas_call(
        functools.partial(gather_kernel, sizes),
        out_shape=(
            jax.ShapeDtypeStruct((half, width), BF16),
            jax.ShapeDtypeStruct(sizes + (seqs, width), BF16),
            jax.ShapeDtypeStruct((count,) + meta.shape, F32),
        ),
        in_specs=[VMEM_SPEC] * 4,
        out_specs=(VMEM_SPEC,) * 3,
        scratch_shapes=[
            pltpu.VMEM((half, width), BF16),
            dma((2,)),
            dma((count,)),
            dma((count,)),
            dma((2,)),
            dma((3, most)),
            dma((3, most)),
            dma((3, most)),
            dma((3, most)),
        ],
        compiler_params=pltpu.CompilerParams(
            collective_id=0, has_side_effects=True, vmem_limit_bytes=VMEM_LIMIT
        ),
        name="gather_tokens",
    )(partial, hidden, gain, meta)


def scatter_kernel(sizes, parts, first, out, total, from_sibling, land0, land1, sems):
    pair_send, pair_recv, send_sem, recv_sem, last_sem = sems
    ep, at, strides = position(sizes)
    tp = lax.axis_index("tp")
    half = first.shape[0]
    mine = pl.ds(pl.multiple_of(tp * half, half), half)
    other = pl.ds(pl.multiple_of((1 - tp) * half, half), half)
    greet_all(sizes[0] * sizes[1] * sizes[2])
    pairs = []
    for z in range(sizes[0]):
        copy = remote(
            parts.at[z, :, :, other],
            from_sibling.at[z],
            pair_send.at[z],
            pair_recv.at[z],
            (ep, 1 - tp),
        )
        copy.start()
        pairs.append(copy)
    per = sizes[1] * sizes[2]
    for z in range(sizes[0]):
        pairs[z].wait()

        def add(b, carry, z=z):
            y, x = b // sizes[2], b % sizes[2]
            total[z, y, x] = (
                parts[z, y, x, mine, :].astype(F32) + from_sibling[z, y, x].astype(F32)
            ).astype(BF16)
            return carry

        lax.fori_loop(0, per, add, 0)

    def run(core, order, lands):
        held = [pl.ds(0, n) for n in sizes]
        for place, d in enumerate(order):
            land = lands[place]
            copies = []
            for k in range(1, sizes[d]):
                goal = (at[d] + k) % sizes[d]
                view = list(held)
                view[d] = pl.ds(goal, 1)
                copy = remote(
                    total.at[tuple(view)],
                    land.at[k - 1],
                    send_sem.at[d, k],
                    recv_sem.at[d, k],
                    (ep + (goal - at[d]) * strides[d], core),
                )
                copy.start()
                copies.append(copy)
            for copy in copies:
                copy.wait()
            held[d] = pl.ds(at[d], 1)
            box = [land.shape[1 + i] for i in range(3)]
            last = place == len(order) - 1
            flat = box[0] * box[1] * box[2]

            def gather_sum(b, carry, land=land, box=box, last=last, fixed=tuple(held)):
                inner = (b // (box[1] * box[2]), b // box[2] % box[1], b % box[2])
                spot = tuple(at[i] if box[i] == 1 else inner[i] for i in range(3))
                value = total[spot].astype(F32)
                for k in range(land.shape[0]):
                    value = value + land[(k,) + inner].astype(F32)
                if last:
                    out[pl.ds(core * half, half), :] = (first[...].astype(F32) + value).astype(BF16)
                else:
                    total[spot] = value.astype(BF16)
                return carry

            lax.fori_loop(0, flat, gather_sum, 0)

    @pl.when(tp == 0)
    def _():
        run(0, (0, 1, 2), land0)

    @pl.when(tp == 1)
    def _():
        run(1, (2, 1, 0), land1)

    swap = remote(out.at[mine], out.at[mine], last_sem.at[0], last_sem.at[1], (ep, 1 - tp))
    swap.start()
    swap.wait()


def landing(sizes, order, half, width):
    box = list(sizes)
    shapes = []
    for d in order:
        box[d] = 1
        shapes.append(pltpu.VMEM((max(1, sizes[d] - 1),) + tuple(box) + (half, width), BF16))
    return shapes


def scatter_sum(sizes, parts, first):
    half, width = first.shape
    most = max(sizes)
    dma = pltpu.SemaphoreType.DMA
    return pl.pallas_call(
        functools.partial(scatter_kernel, sizes),
        out_shape=jax.ShapeDtypeStruct((2 * half, width), BF16),
        in_specs=[VMEM_SPEC] * 2,
        out_specs=VMEM_SPEC,
        scratch_shapes=[
            pltpu.VMEM(sizes + (half, width), BF16),
            pltpu.VMEM(sizes + (half, width), BF16),
            landing(sizes, (0, 1, 2), half, width),
            landing(sizes, (2, 1, 0), half, width),
            [dma((sizes[0],)), dma((sizes[0],)), dma((3, most)), dma((3, most)), dma((2,))],
        ],
        compiler_params=pltpu.CompilerParams(
            collective_id=1, has_side_effects=True, vmem_limit_bytes=VMEM_LIMIT
        ),
        name="scatter_sum",
    )(parts, first)


def shards(
    hidden,
    mix_gain,
    recept_weight,
    key_weight,
    value_weight,
    decay_down,
    decay_up,
    decay_bias,
    rate_down,
    rate_up,
    rate_bias,
    head_gain,
    out_weight,
    memory_state,
    ffn_gain,
    blend_vector,
    dense_gate,
    dense_up,
    dense_down,
    expert_gate,
    expert_up,
    expert_down,
    routing,
    route_scale,
):
    seqs, width = hidden.shape
    count = lax.axis_size("ep")
    sizes = factors_of(count)
    top = routing.shape[1]
    cap = max(2, 2 * seqs * top // count)
    new_state, partial = attention(
        hidden,
        (
            mix_gain[None],
            recept_weight,
            key_weight,
            value_weight,
            decay_down,
            decay_up,
            decay_bias[None],
            rate_down,
            rate_up,
            rate_bias[None],
            head_gain[None],
            out_weight,
        ),
        memory_state,
    )
    meta = jnp.concatenate([routing.T.astype(F32), route_scale.T], axis=0)
    meta = jnp.pad(meta, ((0, -2 * top % 8), (0, -seqs % 128)))
    first, tokens, metas = gather_tokens(sizes, partial, hidden, ffn_gain[None], meta)
    tokens = tokens.reshape(count * seqs, width)

    hit = metas[:, :top, :seqs] == lax.axis_index("ep").astype(F32)
    chosen = jnp.any(hit, axis=1)
    scale_of = jnp.sum(jnp.where(hit, metas[:, top : 2 * top, :seqs], 0.0), axis=1)
    earlier = jnp.arange(seqs)[:, None] < jnp.arange(seqs)[None, :]
    rank = matmul(chosen.astype(BF16), earlier.astype(BF16)).astype(jnp.int32)
    place = jnp.where(chosen, rank + jnp.arange(count, dtype=jnp.int32)[:, None] * cap, -1)
    select = place.reshape(1, -1) == jnp.arange(count * cap, dtype=jnp.int32)[:, None]
    slot_scale = jnp.sum(jnp.where(select, scale_of.reshape(1, -1), 0.0), axis=1, keepdims=True)
    picked = matmul(select.astype(BF16), tokens).astype(BF16)
    expert_act = (silu_of(matmul(picked, expert_gate[0])) * matmul(picked, expert_up[0])).astype(BF16)
    expert_out = (matmul(expert_act, expert_down[0]) * slot_scale).astype(BF16)
    blend = jax.nn.sigmoid(matmul(tokens, blend_vector[:, None]))
    dense_act = (
        silu_of(matmul(tokens, dense_gate)) * matmul(tokens, dense_up) * blend
    ).astype(BF16)
    spread = (place.reshape(-1, 1) == jnp.arange(count * cap, dtype=jnp.int32)[None, :]).astype(BF16)
    parts = matmul(
        jnp.concatenate([spread, dense_act], axis=1),
        jnp.concatenate([expert_out, dense_down], axis=0),
    ).astype(BF16)
    layer_out = scatter_sum(sizes, parts.reshape(sizes + (seqs, width)), first)
    return (layer_out, new_state)


def solution(mesh):
    in_specs = (
        P("ep", None),
        P(),
        P(None, "tp"),
        P(None, "tp"),
        P(None, "tp"),
        P(),
        P(),
        P(),
        P(),
        P(),
        P(),
        P(),
        P("tp", None),
        P("ep", "tp", None, None),
        P(),
        P(),
        P(None, ("ep", "tp")),
        P(None, ("ep", "tp")),
        P(("ep", "tp"), None),
        P("ep", None, "tp"),
        P("ep", None, "tp"),
        P("ep", "tp", None),
        P("ep", None),
        P("ep", None),
    )
    out_specs = (P("ep", None), P("ep", "tp", None, None))
    return jax.shard_map(shards, mesh=mesh, in_specs=in_specs, out_specs=out_specs, check_vma=False)
```

time: 410 us -> 172 us (0.42)
  the two profiles are of different devices: /device:TPU:0 before, /device:TPU:11 now
where the time goes in v1:
time: 172 us
  Pallas kernels  135 us (78%)
  matrix products  25.9 us (15%)
  local copies, waits for them, and re-layouts  7.25 us (4%)
  other arithmetic  3.03 us (2%)
    pallas_call x1, Pallas kernels, scatter_sum(): pl.pallas_call(functools.partial(scatter_kernel, sizes), out_shape=jax.Sh...  51.8 us
    pallas_call x1, Pallas kernels, gather_tokens(): pl.pallas_call(functools.partial(gather_kernel, sizes), out_shape=(jax.Sh...  45.1 us
    pallas_call x1, Pallas kernels, attention(): pl.pallas_call(functools.partial(attention_kernel, step_rows), grid=(seqs...  38 us
    dot_general x8, matrix products, matmul(): return jnp.dot(left, right, preferred_element_type=F32)  25.9 us
    unnamed x16, local copies, waits for them, and re-layouts  6.9 us

profile of v1, /device:TPU:11, one launch (start us, length us, event | category | flops | bytes accessed | tf_op | source)
XLA Modules:
  0.0 171.7 jit_solution(17807946240807696608)
XLA Ops:
  0.6 0.5 iota_multiply_fusion
  1.2 0.7 convert_bitcast_fusion
  1.9 1.3 select_maximum_fusion.meta
  3.1 1.3 reshape.32
  4.4 1.9 %copy.29.decay_down = bf16[2048,64]{1,0:T(8,128)(2,1)} copy(bf16[2048,64]{0,1:T(8,128)(2,1)} %param.29) | data formatting | bytes 524288 | tf_op args[5]
  6.4 2.0 %copy.30.rate_down = bf16[2048,64]{1,0:T(8,128)(2,1)} copy(bf16[2048,64]{0,1:T(8,128)(2,1)} %param.32) | data formatting | bytes 524288 | tf_op args[8]
  8.3 38.0 %attention.1 = (f32[64,8,64,64]{3,2,1,0:T(8,128)}, bf16[64,2048]{1,0:T(8,128)(2,1)}) custom-call(bf16[64,2048]{1,0:T(8,128)(2,1)} %hidden.3, f32[1,2048]{1,0:T(1,128)} %bitcast.46, bf16[2048,512]{1,0:T(8,128)(2,1)} %recept_weight.1, bf16[2048,512]{1,0:T(8,128)(2,1)} %key_weight.1, bf16[2048,512]{1,0:T(8,128)(2,1)} %value_weight.1, ...), custom_call_target="tpu_custom_call" | custom-call | tf_op jit(solution)/shard_map/attention/pallas_call | solution.py:137
  46.3 45.1 %gather_tokens.1 = (bf16[32,2048]{1,0:T(8,128)(2,1)}, bf16[4,2,2,64,2048]{4,3,2,1,0:T(8,128)(2,1)}, f32[16,8,128]{2,1,0:T(8,128)}) custom-call(bf16[64,2048]{1,0:T(8,128)(2,1)} %get-tuple-element.7.partial, bf16[64,2048]{1,0:T(8,128)(2,1)} %hidden.3, f32[1,2048]{1,0:T(1,128)} %bitcast.47, f32[8,128]{1,0:T(8,128)} %select_maximum_fusion.meta), custom_call_target="tpu_custom_call" | custom-call | tf_op jit(solution)/shard_map/gather_tokens/pallas_call | solution.py:303
  91.4 0.0 copy-start.1
  91.4 0.0 copy-start.5
  91.4 0.0 copy-start.2
  91.4 3.4 %fusion.37 = f32[1,1024]{1,0:T(1,128)S(1)} fusion(bf16[1024,2048]{1,0:T(8,128)(2,1)} %bitcast.40, bf16[2048,1]{0,1:T(2,128)(2,1)} %reshape.32), kind=kOutput, calls=%fused_computation.43 | convolution fusion | flops 4194304 | bytes 4202496 | tf_op jit(solution)/shard_map/dot_general | solution.py:19
  94.8 0.0 copy-done.1
  94.9 0.1 broadcast_in_dim.51
  95.0 0.0 copy-done.5
  95.0 0.1 fusion.24
  95.1 0.1 eq.36
  95.2 0.2 select_reduce_fusion
  95.4 0.0 copy-start
  95.4 0.0 copy-start.3
  95.4 0.2 fusion.28
  95.6 0.0 copy-done.2
  95.7 3.9 %fusion.36 = f32[1024,176]{0,1:T(8,128)S(1)} fusion(bf16[1024,2048]{1,0:T(8,128)(2,1)} %bitcast.41, bf16[2048,176]{0,1:T(8,128)(2,1)S(1)} %copy-done.2), kind=kOutput, calls=%fused_computation.42 | convolution fusion | flops 738197504 | bytes 5636096 | tf_op jit(solution)/shard_map/dot_general | solution.py:19
  99.5 1.6 fusion.22
  101.1 1.3 convolution_convert_fusion.1
  102.5 0.2 copy.31
  102.7 3.8 %fusion.4 = f32[256,768]{1,0:T(8,128)} fusion(bf16[256,2048]{1,0:T(8,128)(2,1)S(1)} %convolution_convert_fusion.1, bf16[1,2048,768]{2,1,0:T(8,128)(2,1)} %param.43), kind=kOutput, calls=%fused_computation.5 | convolution fusion | flops 805306368 | bytes 4980736 | tf_op jit(solution)/shard_map/dot_general | solution.py:19
  106.4 6.3 %fusion.9 = bf16[256,2048]{1,0:T(8,128)(2,1)} fusion(bf16[1,768,2048]{2,1,0:T(8,128)(2,1)} %param.45, f32[256]{0:T(256)S(1)} %select_reduce_fusion, bf16[256,2048]{1,0:T(8,128)(2,1)S(1)} %convolution_convert_fusion.1, bf16[1,2048,768]{2,1,0:T(8,128)(2,1)} %param.44, f32[256,768]{1,0:T(8,128)} %fusion.4), kind=kOutput, calls=%fused_computation.8 | convolution fusion | flops 1612644352 | bytes 9176064 | tf_op jit(solution)/shard_map/dot_general | solution.py:19
  112.7 0.0 copy-done.4
  112.7 5.5 %convolution_convert_fusion = bf16[1024,2048]{1,0:T(8,128)(2,1)} fusion(bf16[176,2048]{1,0:T(8,128)(2,1)S(1)} %copy-done.4, bf16[256,2048]{1,0:T(8,128)(2,1)} %fusion.9, bf16[1024,176]{1,0:T(8,128)(2,1)S(1)} %copy.31, bf16[1024,256]{1,0:T(8,128)(2,1)S(1)} %fusion.28), kind=kOutput, calls=%fused_computation | convolution fusion | flops 1819344896 | bytes 6848512 | tf_op jit(solution)/shard_map/dot_general | solution.py:19
  118.2 51.8 %scatter_sum.1 = bf16[64,2048]{1,0:T(8,128)(2,1)} custom-call(bf16[4,2,2,64,2048]{4,3,2,1,0:T(8,128)(2,1)} %bitcast.44, bf16[32,2048]{1,0:T(8,128)(2,1)} %get-tuple-element.10.first), custom_call_target="tpu_custom_call" | custom-call | tf_op jit(solution)/shard_map/scatter_sum/pallas_call | solution.py:427
  170.0 1.7 copy.33
  (6 shorter events, 0.1 us)
Async XLA Ops:
  91.4 3.5 %copy-start.1 = (f32[16,8,128]{2,1,0:T(8,128)S(1)}, f32[16,8,128]{2,1,0:T(8,128)}, u32[]{:S(2)}) copy-start(f32[16,8,128]{2,1,0:T(8,128)} %get-tuple-element.8) | copy-start | bytes 196612
  91.4 3.6 %copy-start.5 = (s32[16]{0:T(128)S(1)}, s32[16]{0:T(128)}, u32[]{:S(2)}) copy-start(s32[16]{0:T(128)} %iota_multiply_fusion) | copy-start | bytes 196
  91.4 4.3 %copy-start.2 = (bf16[2048,176]{0,1:T(8,128)(2,1)S(1)}, bf16[2048,176]{0,1:T(8,128)(2,1)}, u32[]{:S(2)}) copy-start(bf16[2048,176]{0,1:T(8,128)(2,1)} %param.40) | copy-start | bytes 2162692
  95.4 4.1 %copy-start = (bf16[4,2,2,64,2048]{4,3,2,1,0:T(8,128)(2,1)S(1)}, bf16[4,2,2,64,2048]{4,3,2,1,0:T(8,128)(2,1)}, u32[]{:S(2)}) copy-start(bf16[4,2,2,64,2048]{4,3,2,1,0:T(8,128)(2,1)} %get-tuple-element.9) | copy-start | bytes 12582916
  95.4 4.1 %copy-start.3 = (bf16[2048,176]{0,1:T(8,128)(2,1)S(1)}, bf16[2048,176]{0,1:T(8,128)(2,1)}, u32[]{:S(2)}) copy-start(bf16[2048,176]{0,1:T(8,128)(2,1)} %param.41) | copy-start | bytes 2162692
  106.4 6.3 %copy-start.4 = (bf16[176,2048]{1,0:T(8,128)(2,1)S(1)}, bf16[176,2048]{1,0:T(8,128)(2,1)}, u32[]{:S(2)}) copy-start(bf16[176,2048]{1,0:T(8,128)(2,1)} %param.42) | copy-start | bytes 2162692

commit v2 on v1

--- a/solution.py
+++ b/solution.py
@@ -17,6 +17,10 @@
 
 def matmul(left, right):
     return jnp.dot(left, right, preferred_element_type=F32)
+
+
+def matmul_nt(left, right):
+    return lax.dot_general(left, right, (((1,), (1,)), ((), ())), preferred_element_type=F32)
 
 
 def silu_of(tensor):
@@ -74,11 +78,11 @@
         recept = matmul(normed, recept_weight[...]).astype(BF16).astype(F32)
         keys = matmul(normed, key_weight[...]).astype(BF16).astype(F32)
         vals = matmul(normed, value_weight[...]).astype(BF16).astype(F32)
-        decay_low = jnp.tanh(matmul(normed, decay_down[...])).astype(BF16)
+        decay_low = jnp.tanh(matmul_nt(normed, decay_down[...])).astype(BF16)
         decay_pre = matmul(decay_low, decay_up[:, own]) + decay_bias[:, own]
         softplus = jnp.maximum(-decay_pre, 0.0) + jnp.log1p(jnp.exp(-jnp.abs(decay_pre)))
         decay = jnp.exp(-jnp.exp(-softplus - 0.5))
-        rate_low = matmul(normed, rate_down[...]).astype(BF16)
+        rate_low = matmul_nt(normed, rate_down[...]).astype(BF16)
         rate = 1.0 / (1.0 + jnp.exp(-(matmul(rate_low, rate_up[:, own]) + rate_bias[:, own])))
         for h in range(heads):
             cols = slice(h * size, (h + 1) * size)
@@ -91,25 +95,31 @@
             value_s[h] = vals[:, cols]
             decay_s[h] = decay[:, cols]
 
-    eye = (
-        lax.broadcasted_iota(jnp.int32, (size, size), 0)
-        == lax.broadcasted_iota(jnp.int32, (size, size), 1)
-    ).astype(F32)
+    tall = (16, size)
+    place = lax.broadcasted_iota(jnp.int32, tall, 0)
+
+    def wide(row):
+        return jnp.broadcast_to(row, tall)
 
     def one_sequence(local, carry):
         row = pl.ds(step * step_rows + local, 1)
         for h in range(heads):
             state = state_in[local, h]
-            removed = jnp.sum(state * unit_s[h, row], axis=-1, keepdims=True)
-            value = jnp.sum(eye * value_s[h, row], axis=-1, keepdims=True)
-            new = (
-                state * decay_s[h, row]
-                - removed * unit_rate_s[h, row]
-                + value * key_rate_s[h, row]
+            removed = matmul_nt(wide(unit_s[h, row]).astype(BF16), state.astype(BF16))
+            left = jnp.where(place == 0, -removed, wide(value_s[h, row])).astype(BF16)
+            key_rate = wide(key_rate_s[h, row])
+            rest = key_rate - key_rate.astype(BF16).astype(F32)
+            right = jnp.where(
+                place == 0,
+                wide(unit_rate_s[h, row]),
+                jnp.where(place == 1, key_rate, jnp.where(place == 2, rest, 0.0)),
+            ).astype(BF16)
+            new = state * decay_s[h, row] + lax.dot_general(
+                left, right, (((0,), (0,)), ((), ())), preferred_element_type=F32
             )
             state_out[local, h] = new
-            out = jnp.sum(new * recept_s[h, row], axis=-1, keepdims=True)
-            readout_s[h, row] = jnp.sum(eye * out, axis=0, keepdims=True)
+            out = matmul_nt(wide(recept_s[h, row]).astype(BF16), new.astype(BF16))
+            readout_s[h, row] = out[0:1]
         return carry
 
     lax.fori_loop(0, step_rows, one_sequence, 0)
@@ -196,7 +206,6 @@
     part_sem,
     meta_send,
     meta_recv,
-    own_sem,
     send_sem,
     recv_sem,
     pass_send,
@@ -233,59 +242,87 @@
     ffn_in = rms_scaled(total.astype(F32), gain[...]).astype(BF16)
     tokens[at[0], at[1], at[2], mine, :] = ffn_in
 
-    def blocks(order):
-        held = [pl.ds(c, 1) for c in at]
-        for d in order:
-            before = tuple(held)
-            for k in range(1, sizes[d]):
-                come = list(held)
-                come[d] = pl.ds((at[d] + sizes[d] - k) % sizes[d], 1)
-                yield d, k, before, tuple(come)
-            held[d] = pl.ds(0, sizes[d])
+    def views(order, r):
+        _, d2, d3 = order
+
+        def view(k, second, third):
+            spot = [pl.ds((at[0] + sizes[0] - k) % sizes[0], 1), None, None]
+            spot[d2], spot[d3] = second, third
+            return tokens.at[tuple(spot) + (r,)]
+
+        def one(d, j=0):
+            return pl.ds((at[d] + sizes[d] - j) % sizes[d], 1)
+
+        whole = pl.ds(0, sizes[d2])
+        return (
+            lambda k, j=0: view(k, one(d2), one(d3)),
+            lambda k, j=0: view(k, one(d2, j), one(d3)),
+            lambda k, j=0: view(k, whole, one(d3, j)),
+        )
 
     def run(core, order, order_of_other):
-        rows = pl.ds(core * half, half)
-        rows_of_other = pl.ds((1 - core) * half, half)
         sibling = (ep, 1 - core)
-
-        def own_copy(r):
-            view = tokens.at[pl.ds(at[0], 1), pl.ds(at[1], 1), pl.ds(at[2], 1), r]
-            return remote(view, view, own_sem.at[0], own_sem.at[1], sibling)
-
-        def pass_copy(d, k, come, r):
-            view = tokens.at[come + (r,)]
-            return remote(view, view, pass_send.at[d, k], pass_recv.at[d, k], sibling)
-
-        to_wait = [own_copy(rows)]
-        to_wait[0].start()
-        steps = list(blocks(order))
-        for d in order:
-            copies = []
-            for dd, k, before, come in steps:
-                if dd == d:
-                    peer = ep + ((at[d] + k) % sizes[d] - at[d]) * strides[d]
-                    view = tokens.at[before + (rows,)]
-                    copy = remote(view, view, send_sem.at[d, k], recv_sem.at[d, k], (peer, core))
-                    copy.start()
-                    copies.append((copy, k, come))
-            for copy, k, come in copies:
-                copy.wait()
-                onward = pass_copy(d, k, come, rows)
-                onward.start()
-                to_wait.append(onward)
-        for copy in to_wait:
+        come = views(order, pl.ds(core * half, half))
+        chunks = sizes[0]
+        flights, passed = {}, []
+
+        def send(stage, k, j):
+            d = order[stage]
+            source = come[stage](0 if stage == 0 else k)
+            peer = ep + ((at[d] + j) % sizes[d] - at[d]) * strides[d]
+            slot = (stage, k, j if stage else 0)
+            copy = remote(source, source, send_sem.at[slot], recv_sem.at[slot], (peer, core))
+            copy.start()
+            flights[slot] = copy
+
+        def onward(stage, k, j):
+            view = come[stage](k, j)
+            slot = (stage, k, j)
+            copy = remote(view, view, pass_send.at[slot], pass_recv.at[slot], sibling)
+            copy.start()
+            passed.append(copy)
+
+        def first_phase(k):
+            if k:
+                flights[0, k, 0].wait()
+            for j in range(1, sizes[order[1]]):
+                send(1, k, j)
+            onward(0, k, 0)
+
+        def later_phase(stage, k):
+            for j in range(1, sizes[order[stage]]):
+                flights[stage, k, j].wait()
+            if stage == 1:
+                for j in range(1, sizes[order[2]]):
+                    send(2, k, j)
+            for j in range(1, sizes[order[stage]]):
+                onward(stage, k, j)
+
+        for k in range(1, chunks):
+            send(0, k, k)
+        for t in range(chunks + 2):
+            if 0 <= t - 1 < chunks:
+                later_phase(1, t - 1)
+            if t < chunks:
+                first_phase(t)
+            if 0 <= t - 2 < chunks:
+                later_phase(2, t - 2)
+        for copy in passed:
             copy.wait_send()
-        own_copy(rows_of_other).wait_recv()
-        for d, k, before, come in blocks(order_of_other):
-            pass_copy(d, k, come, rows_of_other).wait_recv()
+        theirs = views(order_of_other, pl.ds((1 - core) * half, half))
+        for stage in range(3):
+            for k in range(chunks):
+                for j in range(1, sizes[order_of_other[stage]]) if stage else (0,):
+                    view, slot = theirs[stage](k, j), (stage, k, j)
+                    remote(view, view, pass_send.at[slot], pass_recv.at[slot], sibling).wait_recv()
 
     @pl.when(tp == 0)
     def _():
-        run(0, (2, 1, 0), (0, 1, 2))
+        run(0, (0, 2, 1), (0, 1, 2))
 
     @pl.when(tp == 1)
     def _():
-        run(1, (0, 1, 2), (2, 1, 0))
+        run(1, (0, 1, 2), (0, 2, 1))
 
     def wait_meta(k, carry):
         meta_copy(k).wait()
@@ -314,11 +351,10 @@
             dma((2,)),
             dma((count,)),
             dma((count,)),
-            dma((2,)),
-            dma((3, most)),
-            dma((3, most)),
-            dma((3, most)),
-            dma((3, most)),
+            dma((3, sizes[0], most)),
+            dma((3, sizes[0], most)),
+            dma((3, sizes[0], most)),
+            dma((3, sizes[0], most)),
         ],
         compiler_params=pltpu.CompilerParams(
             collective_id=0, has_side_effects=True, vmem_limit_bytes=VMEM_LIMIT
@@ -334,90 +370,114 @@
     half = first.shape[0]
     mine = pl.ds(pl.multiple_of(tp * half, half), half)
     other = pl.ds(pl.multiple_of((1 - tp) * half, half), half)
+    chunks = sizes[0]
+    goals = [(at[0] + 1 + k) % chunks for k in range(chunks)]
     greet_all(sizes[0] * sizes[1] * sizes[2])
     pairs = []
-    for z in range(sizes[0]):
+    for k in range(chunks):
         copy = remote(
-            parts.at[z, :, :, other],
-            from_sibling.at[z],
-            pair_send.at[z],
-            pair_recv.at[z],
+            parts.at[goals[k], :, :, other],
+            from_sibling.at[k],
+            pair_send.at[k],
+            pair_recv.at[k],
             (ep, 1 - tp),
         )
         copy.start()
         pairs.append(copy)
-    per = sizes[1] * sizes[2]
-    for z in range(sizes[0]):
-        pairs[z].wait()
-
-        def add(b, carry, z=z):
-            y, x = b // sizes[2], b % sizes[2]
-            total[z, y, x] = (
-                parts[z, y, x, mine, :].astype(F32) + from_sibling[z, y, x].astype(F32)
-            ).astype(BF16)
-            return carry
-
-        lax.fori_loop(0, per, add, 0)
-
-    def run(core, order, lands):
-        held = [pl.ds(0, n) for n in sizes]
-        for place, d in enumerate(order):
-            land = lands[place]
-            copies = []
-            for k in range(1, sizes[d]):
-                goal = (at[d] + k) % sizes[d]
-                view = list(held)
-                view[d] = pl.ds(goal, 1)
-                copy = remote(
-                    total.at[tuple(view)],
-                    land.at[k - 1],
-                    send_sem.at[d, k],
-                    recv_sem.at[d, k],
-                    (ep + (goal - at[d]) * strides[d], core),
-                )
-                copy.start()
-                copies.append(copy)
-            for copy in copies:
-                copy.wait()
-            held[d] = pl.ds(at[d], 1)
-            box = [land.shape[1 + i] for i in range(3)]
-            last = place == len(order) - 1
-            flat = box[0] * box[1] * box[2]
-
-            def gather_sum(b, carry, land=land, box=box, last=last, fixed=tuple(held)):
-                inner = (b // (box[1] * box[2]), b // box[2] % box[1], b % box[2])
-                spot = tuple(at[i] if box[i] == 1 else inner[i] for i in range(3))
-                value = total[spot].astype(F32)
-                for k in range(land.shape[0]):
-                    value = value + land[(k,) + inner].astype(F32)
-                if last:
-                    out[pl.ds(core * half, half), :] = (first[...].astype(F32) + value).astype(BF16)
-                else:
-                    total[spot] = value.astype(BF16)
+
+    def run(core, d1, d2, lands):
+        rows = pl.ds(core * half, half)
+        flights = {}
+
+        def spot(k, c1, c2):
+            place = [goals[k], None, None]
+            place[d1], place[d2] = c1, c2
+            return tuple(place)
+
+        def send(stage, k, j, source, dst, d):
+            peer = ep + ((at[d] + j) % sizes[d] - at[d]) * strides[d]
+            slot = (stage, k, j if stage < 2 else 0)
+            copy = remote(source, dst, send_sem.at[slot], recv_sem.at[slot], (peer, core))
+            copy.start()
+            flights[slot] = copy
+
+        def pair_sum(k):
+            pairs[k].wait()
+
+            def add(b, carry):
+                y, x = b // sizes[2], b % sizes[2]
+                total[goals[k], y, x] = (
+                    parts[goals[k], y, x, rows, :].astype(F32) + from_sibling[k, y, x].astype(F32)
+                ).astype(BF16)
                 return carry
 
-            lax.fori_loop(0, flat, gather_sum, 0)
+            lax.fori_loop(0, sizes[1] * sizes[2], add, 0)
+            for j in range(1, sizes[d1]):
+                source = total.at[spot(k, (at[d1] + j) % sizes[d1], slice(None))]
+                send(0, k, j, source, lands[0].at[k, j - 1], d1)
+
+        def first_sum(k):
+            for j in range(1, sizes[d1]):
+                flights[0, k, j].wait()
+
+            def add(b, carry):
+                place = spot(k, at[d1], b)
+                value = total[place].astype(F32)
+                for j in range(1, sizes[d1]):
+                    value = value + lands[0][k, j - 1, b].astype(F32)
+                total[place] = value.astype(BF16)
+                return carry
+
+            lax.fori_loop(0, sizes[d2], add, 0)
+            for j in range(1, sizes[d2]):
+                source = total.at[spot(k, at[d1], (at[d2] + j) % sizes[d2])]
+                send(1, k, j, source, lands[1].at[k, j - 1], d2)
+
+        def second_sum(k):
+            for j in range(1, sizes[d2]):
+                flights[1, k, j].wait()
+            place = spot(k, at[d1], at[d2])
+            value = total[place].astype(F32)
+            for j in range(1, sizes[d2]):
+                value = value + lands[1][k, j - 1].astype(F32)
+            if k < chunks - 1:
+                total[place] = value.astype(BF16)
+                send(2, k, k + 1, total.at[place], lands[2].at[k], 0)
+                return
+            value = value + first[...].astype(F32)
+            for i in range(chunks - 1):
+                flights[2, i, 0].wait()
+                value = value + lands[2][i].astype(F32)
+            out[rows, :] = value.astype(BF16)
+
+        for t in range(chunks + 2):
+            if t < chunks:
+                pair_sum(t)
+            if 0 <= t - 1 < chunks:
+                first_sum(t - 1)
+            if 0 <= t - 2 < chunks:
+                second_sum(t - 2)
 
     @pl.when(tp == 0)
     def _():
-        run(0, (0, 1, 2), land0)
+        run(0, 1, 2, land0)
 
     @pl.when(tp == 1)
     def _():
-        run(1, (2, 1, 0), land1)
+        run(1, 2, 1, land1)
 
     swap = remote(out.at[mine], out.at[mine], last_sem.at[0], last_sem.at[1], (ep, 1 - tp))
     swap.start()
     swap.wait()
 
 
-def landing(sizes, order, half, width):
-    box = list(sizes)
-    shapes = []
-    for d in order:
-        box[d] = 1
-        shapes.append(pltpu.VMEM((max(1, sizes[d] - 1),) + tuple(box) + (half, width), BF16))
-    return shapes
+def landing(sizes, d1, d2, half, width):
+    chunks, block = sizes[0], (half, width)
+    return [
+        pltpu.VMEM((chunks, max(1, sizes[d1] - 1), sizes[d2]) + block, BF16),
+        pltpu.VMEM((chunks, max(1, sizes[d2] - 1)) + block, BF16),
+        pltpu.VMEM((max(1, chunks - 1),) + block, BF16),
+    ]
 
 
 def scatter_sum(sizes, parts, first):
@@ -432,9 +492,15 @@
         scratch_shapes=[
             pltpu.VMEM(sizes + (half, width), BF16),
             pltpu.VMEM(sizes + (half, width), BF16),
-            landing(sizes, (0, 1, 2), half, width),
-            landing(sizes, (2, 1, 0), half, width),
-            [dma((sizes[0],)), dma((sizes[0],)), dma((3, most)), dma((3, most)), dma((2,))],
+            landing(sizes, 1, 2, half, width),
+            landing(sizes, 2, 1, half, width),
+            [
+                dma((sizes[0],)),
+                dma((sizes[0],)),
+                dma((3, sizes[0], most)),
+                dma((3, sizes[0], most)),
+                dma((2,)),
+            ],
         ],
         compiler_params=pltpu.CompilerParams(
             collective_id=1, has_side_effects=True, vmem_limit_bytes=VMEM_LIMIT
@@ -481,10 +547,10 @@
             recept_weight,
             key_weight,
             value_weight,
-            decay_down,
+            decay_down.T,
             decay_up,
             decay_bias[None],
-            rate_down,
+            rate_down.T,
             rate_up,
             rate_bias[None],
             head_gain[None],
@@ -508,7 +574,7 @@
     picked = matmul(select.astype(BF16), tokens).astype(BF16)
     expert_act = (silu_of(matmul(picked, expert_gate[0])) * matmul(picked, expert_up[0])).astype(BF16)
     expert_out = (matmul(expert_act, expert_down[0]) * slot_scale).astype(BF16)
-    blend = jax.nn.sigmoid(matmul(tokens, blend_vector[:, None]))
+    blend = jax.nn.sigmoid(matmul_nt(tokens, blend_vector[None]))
     dense_act = (
         silu_of(matmul(tokens, dense_gate)) * matmul(tokens, dense_up) * blend
     ).astype(BF16)

time: 172 us -> 212 us (1.23)
  the two profiles are of different devices: /device:TPU:11 before, /device:TPU:0 now
where the time goes in v2:
time: 212 us
  Pallas kernels  179 us (84%)
  matrix products  25.9 us (12%)
  local copies, waits for them, and re-layouts  3.33 us (2%)
  other arithmetic  3.03 us (1%)
    pallas_call x1, Pallas kernels, attention(): pl.pallas_call(functools.partial(attention_kernel, step_rows), grid=(seqs...  104 us
    pallas_call x1, Pallas kernels, gather_tokens(): pl.pallas_call(functools.partial(gather_kernel, sizes), out_shape=(jax.Sh...  40.5 us
    pallas_call x1, Pallas kernels, scatter_sum(): pl.pallas_call(functools.partial(scatter_kernel, sizes), out_shape=jax.Sh...  34.5 us
    dot_general x7, matrix products, matmul(): return jnp.dot(left, right, preferred_element_type=F32)  22.4 us

profile of v2, /device:TPU:0, one launch (start us, length us, event | category | flops | bytes accessed | tf_op | source)
XLA Modules:
  0.0 211.8 jit_solution(5912695164037811966)
XLA Ops:
  0.6 0.5 iota_multiply_fusion
  1.2 0.7 convert_bitcast_fusion
  1.9 1.3 select_maximum_fusion.meta
  3.1 1.3 reshape.32
  4.4 103.9 %attention.1 = (f32[64,8,64,64]{3,2,1,0:T(8,128)}, bf16[64,2048]{1,0:T(8,128)(2,1)}) custom-call(bf16[64,2048]{1,0:T(8,128)(2,1)} %hidden.3, f32[1,2048]{1,0:T(1,128)} %bitcast.50, bf16[2048,512]{1,0:T(8,128)(2,1)} %recept_weight.1, bf16[2048,512]{1,0:T(8,128)(2,1)} %key_weight.1, bf16[2048,512]{1,0:T(8,128)(2,1)} %value_weight.1, ...), custom_call_target="tpu_custom_call" | custom-call | tf_op jit(solution)/shard_map/attention/pallas_call | solution.py:147
  108.3 40.5 %gather_tokens.1 = (bf16[32,2048]{1,0:T(8,128)(2,1)}, bf16[4,2,2,64,2048]{4,3,2,1,0:T(8,128)(2,1)}, f32[16,8,128]{2,1,0:T(8,128)}) custom-call(bf16[64,2048]{1,0:T(8,128)(2,1)} %get-tuple-element.7.partial, bf16[64,2048]{1,0:T(8,128)(2,1)} %hidden.3, f32[1,2048]{1,0:T(1,128)} %bitcast.51, f32[8,128]{1,0:T(8,128)} %select_maximum_fusion.meta), custom_call_target="tpu_custom_call" | custom-call | tf_op jit(solution)/shard_map/gather_tokens/pallas_call | solution.py:340
  148.8 0.0 copy-start.1
  148.8 0.0 copy-start.5
  148.8 0.0 copy-start.2
  148.8 3.4 %fusion.37 = f32[1,1024]{1,0:T(1,128)S(1)} fusion(bf16[1024,2048]{1,0:T(8,128)(2,1)} %bitcast.42, bf16[2048,1]{0,1:T(2,128)(2,1)} %reshape.32), kind=kOutput, calls=%fused_computation.43 | convolution fusion | flops 4194304 | bytes 4202496 | tf_op jit(solution)/shard_map/dot_general | solution.py:23
  152.3 0.0 copy-done.1
  152.4 0.1 broadcast_in_dim.51
  152.4 0.0 copy-done.5
  152.4 0.1 fusion.24
  152.5 0.1 eq.36
  152.6 0.2 select_reduce_fusion
  152.8 0.0 copy-start
  152.8 0.0 copy-start.3
  152.9 0.2 fusion.28
  153.1 0.0 copy-done.2
  153.1 3.9 %fusion.36 = f32[1024,176]{0,1:T(8,128)S(1)} fusion(bf16[1024,2048]{1,0:T(8,128)(2,1)} %bitcast.43, bf16[2048,176]{0,1:T(8,128)(2,1)S(1)} %copy-done.2), kind=kOutput, calls=%fused_computation.42 | convolution fusion | flops 738197504 | bytes 5636096 | tf_op jit(solution)/shard_map/dot_general | solution.py:19
  157.0 0.0 copy-done
  157.0 0.0 copy-done.3
  157.0 1.6 fusion.22
  158.6 1.3 convolution_convert_fusion.1
  159.9 0.2 copy.27
  160.1 3.8 %fusion.4 = f32[256,768]{1,0:T(8,128)} fusion(bf16[256,2048]{1,0:T(8,128)(2,1)S(1)} %convolution_convert_fusion.1, bf16[1,2048,768]{2,1,0:T(8,128)(2,1)} %param.43), kind=kOutput, calls=%fused_computation.5 | convolution fusion | flops 805306368 | bytes 4980736 | tf_op jit(solution)/shard_map/dot_general | solution.py:19
  163.9 6.3 %fusion.9 = bf16[256,2048]{1,0:T(8,128)(2,1)} fusion(bf16[1,768,2048]{2,1,0:T(8,128)(2,1)} %param.45, f32[256]{0:T(256)S(1)} %select_reduce_fusion, bf16[256,2048]{1,0:T(8,128)(2,1)S(1)} %convolution_convert_fusion.1, bf16[1,2048,768]{2,1,0:T(8,128)(2,1)} %param.44, f32[256,768]{1,0:T(8,128)} %fusion.4), kind=kOutput, calls=%fused_computation.8 | convolution fusion | flops 1612644352 | bytes 9176064 | tf_op jit(solution)/shard_map/dot_general | solution.py:19
  170.2 0.0 copy-done.4
  170.2 5.5 %convolution_convert_fusion = bf16[1024,2048]{1,0:T(8,128)(2,1)} fusion(bf16[176,2048]{1,0:T(8,128)(2,1)S(1)} %copy-done.4, bf16[256,2048]{1,0:T(8,128)(2,1)} %fusion.9, bf16[1024,176]{1,0:T(8,128)(2,1)S(1)} %copy.27, bf16[1024,256]{1,0:T(8,128)(2,1)S(1)} %fusion.28), kind=kOutput, calls=%fused_computation | convolution fusion | flops 1819344896 | bytes 6848512 | tf_op jit(solution)/shard_map/dot_general | solution.py:19
  175.7 34.5 %scatter_sum.1 = bf16[64,2048]{1,0:T(8,128)(2,1)} custom-call(bf16[4,2,2,64,2048]{4,3,2,1,0:T(8,128)(2,1)} %bitcast.46, bf16[32,2048]{1,0:T(8,128)(2,1)} %get-tuple-element.10.first), custom_call_target="tpu_custom_call" | custom-call | tf_op jit(solution)/shard_map/scatter_sum/pallas_call | solution.py:487
  210.2 1.7 copy.29
  (4 shorter events, 0.1 us)
Async XLA Ops:
  148.8 3.5 %copy-start.1 = (f32[16,8,128]{2,1,0:T(8,128)S(1)}, f32[16,8,128]{2,1,0:T(8,128)}, u32[]{:S(2)}) copy-start(f32[16,8,128]{2,1,0:T(8,128)} %get-tuple-element.8) | copy-start | bytes 196612
  148.8 3.6 %copy-start.5 = (s32[16]{0:T(128)S(1)}, s32[16]{0:T(128)}, u32[]{:S(2)}) copy-start(s32[16]{0:T(128)} %iota_multiply_fusion) | copy-start | bytes 196
  148.8 4.3 %copy-start.2 = (bf16[2048,176]{0,1:T(8,128)(2,1)S(1)}, bf16[2048,176]{0,1:T(8,128)(2,1)}, u32[]{:S(2)}) copy-start(bf16[2048,176]{0,1:T(8,128)(2,1)} %param.40) | copy-start | bytes 2162692
  152.8 4.1 %copy-start = (bf16[4,2,2,64,2048]{4,3,2,1,0:T(8,128)(2,1)S(1)}, bf16[4,2,2,64,2048]{4,3,2,1,0:T(8,128)(2,1)}, u32[]{:S(2)}) copy-start(bf16[4,2,2,64,2048]{4,3,2,1,0:T(8,128)(2,1)} %get-tuple-element.9) | copy-start | bytes 12582916
  152.8 4.1 %copy-start.3 = (bf16[2048,176]{0,1:T(8,128)(2,1)S(1)}, bf16[2048,176]{0,1:T(8,128)(2,1)}, u32[]{:S(2)}) copy-start(bf16[2048,176]{0,1:T(8,128)(2,1)} %param.41) | copy-start | bytes 2162692
  163.9 6.3 %copy-start.4 = (bf16[176,2048]{1,0:T(8,128)(2,1)S(1)}, bf16[176,2048]{1,0:T(8,128)(2,1)}, u32[]{:S(2)}) copy-start(bf16[176,2048]{1,0:T(8,128)(2,1)} %param.42) | copy-start | bytes 2162692

commit v3 on v2

--- a/solution.py
+++ b/solution.py
@@ -95,34 +95,27 @@
             value_s[h] = vals[:, cols]
             decay_s[h] = decay[:, cols]
 
-    tall = (16, size)
-    place = lax.broadcasted_iota(jnp.int32, tall, 0)
-
-    def wide(row):
-        return jnp.broadcast_to(row, tall)
+    shape, flat = (heads, size, size), (heads * size, size)
+    eye = lax.broadcasted_iota(jnp.int32, shape, 1) == lax.broadcasted_iota(jnp.int32, shape, 2)
+    ones = jnp.ones((size, size), BF16)
+
+    def row_sums(values):
+        return matmul(values.astype(BF16).reshape(flat), ones).reshape(shape)
 
     def one_sequence(local, carry):
         row = pl.ds(step * step_rows + local, 1)
-        for h in range(heads):
-            state = state_in[local, h]
-            removed = matmul_nt(wide(unit_s[h, row]).astype(BF16), state.astype(BF16))
-            left = jnp.where(place == 0, -removed, wide(value_s[h, row])).astype(BF16)
-            key_rate = wide(key_rate_s[h, row])
-            rest = key_rate - key_rate.astype(BF16).astype(F32)
-            right = jnp.where(
-                place == 0,
-                wide(unit_rate_s[h, row]),
-                jnp.where(place == 1, key_rate, jnp.where(place == 2, rest, 0.0)),
-            ).astype(BF16)
-            new = state * decay_s[h, row] + lax.dot_general(
-                left, right, (((0,), (0,)), ((), ())), preferred_element_type=F32
-            )
-            state_out[local, h] = new
-            out = matmul_nt(wide(recept_s[h, row]).astype(BF16), new.astype(BF16))
-            readout_s[h, row] = out[0:1]
+        state = state_in[local]
+        removed = row_sums(state * unit_s[:, row])
+        value = row_sums(jnp.where(eye, value_s[:, row], 0.0))
+        new = (
+            state * decay_s[:, row] - removed * unit_rate_s[:, row] + value * key_rate_s[:, row]
+        )
+        state_out[local] = new
+        out = row_sums(new * recept_s[:, row])
+        readout_s[:, row] = jnp.sum(jnp.where(eye, out, 0.0), axis=1, keepdims=True)
         return carry
 
-    lax.fori_loop(0, step_rows, one_sequence, 0)
+    lax.fori_loop(0, step_rows, one_sequence, 0, unroll=4)
 
     @pl.when(step == pl.num_programs(0) - 1)
     def _():
@@ -298,12 +291,13 @@
             for j in range(1, sizes[order[stage]]):
                 onward(stage, k, j)
 
+        first_phase(0)
         for k in range(1, chunks):
             send(0, k, k)
         for t in range(chunks + 2):
             if 0 <= t - 1 < chunks:
                 later_phase(1, t - 1)
-            if t < chunks:
+            if 0 < t < chunks:
                 first_phase(t)
             if 0 <= t - 2 < chunks:
                 later_phase(2, t - 2)

time: 212 us -> 134 us (0.63)
  Pallas kernels: 179 us -> 101 us
    pallas_call x1, Pallas kernels: 104 us -> 25.7 us  [attention(): pl.pallas_call(functools.partial(attention_kernel, step_rows), grid=(seqs...]
where the time goes in v3:
time: 134 us
  Pallas kernels  101 us (75%)
  matrix products  25.8 us (19%)
  local copies, waits for them, and re-layouts  3.33 us (2%)
  other arithmetic  3.03 us (2%)
    pallas_call x1, Pallas kernels, gather_tokens(): pl.pallas_call(functools.partial(gather_kernel, sizes), out_shape=(jax.Sh...  40.5 us
    pallas_call x1, Pallas kernels, scatter_sum(): pl.pallas_call(functools.partial(scatter_kernel, sizes), out_shape=jax.Sh...  34.5 us
    pallas_call x1, Pallas kernels, attention(): pl.pallas_call(functools.partial(attention_kernel, step_rows), grid=(seqs...  25.7 us
    dot_general x7, matrix products, matmul(): return jnp.dot(left, right, preferred_element_type=F32)  22.4 us
    dot_general x1, matrix products, matmul_nt(): lax.dot_general(left, right, (((1,), (1,)), ((), ())), preferred_element_...  3.44 us
    unnamed x14, local copies, waits for them, and re-layouts  2.99 us

profile of v3, /device:TPU:0, one launch (start us, length us, event | category | flops | bytes accessed | tf_op | source)
XLA Modules:
  0.0 133.8 jit_solution(7443754944604411382)
XLA Ops:
  0.6 0.5 iota_multiply_fusion
  1.2 0.7 convert_bitcast_fusion
  1.9 1.3 select_maximum_fusion.meta
  3.1 1.3 reshape.32
  4.4 25.7 %attention.1 = (f32[64,8,64,64]{3,2,1,0:T(8,128)}, bf16[64,2048]{1,0:T(8,128)(2,1)}) custom-call(bf16[64,2048]{1,0:T(8,128)(2,1)} %hidden.3, f32[1,2048]{1,0:T(1,128)} %bitcast.50, bf16[2048,512]{1,0:T(8,128)(2,1)} %recept_weight.1, bf16[2048,512]{1,0:T(8,128)(2,1)} %key_weight.1, bf16[2048,512]{1,0:T(8,128)(2,1)} %value_weight.1, ...), custom_call_target="tpu_custom_call" | custom-call | tf_op jit(solution)/shard_map/attention/pallas_call | solution.py:140
  30.2 40.5 %gather_tokens.1 = (bf16[32,2048]{1,0:T(8,128)(2,1)}, bf16[4,2,2,64,2048]{4,3,2,1,0:T(8,128)(2,1)}, f32[16,8,128]{2,1,0:T(8,128)}) custom-call(bf16[64,2048]{1,0:T(8,128)(2,1)} %get-tuple-element.7.partial, bf16[64,2048]{1,0:T(8,128)(2,1)} %hidden.3, f32[1,2048]{1,0:T(1,128)} %bitcast.51, f32[8,128]{1,0:T(8,128)} %select_maximum_fusion.meta), custom_call_target="tpu_custom_call" | custom-call | tf_op jit(solution)/shard_map/gather_tokens/pallas_call | solution.py:334
  70.7 0.0 copy-start.1
  70.7 0.0 copy-start.5
  70.7 0.0 copy-start.2
  70.7 3.4 %fusion.37 = f32[1,1024]{1,0:T(1,128)S(1)} fusion(bf16[1024,2048]{1,0:T(8,128)(2,1)} %bitcast.42, bf16[2048,1]{0,1:T(2,128)(2,1)} %reshape.32), kind=kOutput, calls=%fused_computation.43 | convolution fusion | flops 4194304 | bytes 4202496 | tf_op jit(solution)/shard_map/dot_general | solution.py:23
  74.1 0.0 copy-done.1
  74.2 0.1 broadcast_in_dim.51
  74.3 0.0 copy-done.5
  74.3 0.1 fusion.24
  74.4 0.1 eq.36
  74.5 0.2 select_reduce_fusion
  74.7 0.0 copy-start
  74.7 0.0 copy-start.3
  74.7 0.2 fusion.28
  74.9 0.0 copy-done.2
  75.0 3.9 %fusion.36 = f32[1024,176]{0,1:T(8,128)S(1)} fusion(bf16[1024,2048]{1,0:T(8,128)(2,1)} %bitcast.43, bf16[2048,176]{0,1:T(8,128)(2,1)S(1)} %copy-done.2), kind=kOutput, calls=%fused_computation.42 | convolution fusion | flops 738197504 | bytes 5636096 | tf_op jit(solution)/shard_map/dot_general | solution.py:19
  78.8 0.0 copy-done
  78.8 0.0 copy-done.3
  78.9 1.6 %fusion.22 = bf16[1024,176]{0,1:T(8,128)(2,1)S(1)} fusion(bf16[1024,2048]{1,0:T(8,128)(2,1)S(1)} %bitcast.44, bf16[2048,176]{0,1:T(8,128)(2,1)S(1)} %copy-done.3, f32[1024,176]{0,1:T(8,128)S(1)} %fusion.36, f32[1024]{0:T(1024)S(1)} %add_divide_fusion), kind=kOutput, calls=%fused_computation.17 | convolution fusion | flops 739278848 | bytes 6000640 | tf_op jit(solution)/shard_map/dot_general | solution.py:19
  80.5 1.3 convolution_convert_fusion.1
  81.8 0.2 copy.27
  82.0 3.8 %fusion.4 = f32[256,768]{1,0:T(8,128)} fusion(bf16[256,2048]{1,0:T(8,128)(2,1)S(1)} %convolution_convert_fusion.1, bf16[1,2048,768]{2,1,0:T(8,128)(2,1)} %param.43), kind=kOutput, calls=%fused_computation.5 | convolution fusion | flops 805306368 | bytes 4980736 | tf_op jit(solution)/shard_map/dot_general | solution.py:19
  85.8 6.3 %fusion.9 = bf16[256,2048]{1,0:T(8,128)(2,1)} fusion(bf16[1,768,2048]{2,1,0:T(8,128)(2,1)} %param.45, f32[256]{0:T(256)S(1)} %select_reduce_fusion, bf16[256,2048]{1,0:T(8,128)(2,1)S(1)} %convolution_convert_fusion.1, bf16[1,2048,768]{2,1,0:T(8,128)(2,1)} %param.44, f32[256,768]{1,0:T(8,128)} %fusion.4), kind=kOutput, calls=%fused_computation.8 | convolution fusion | flops 1612644352 | bytes 9176064 | tf_op jit(solution)/shard_map/dot_general | solution.py:19
  92.0 0.0 copy-done.4
  92.0 5.5 %convolution_convert_fusion = bf16[1024,2048]{1,0:T(8,128)(2,1)} fusion(bf16[176,2048]{1,0:T(8,128)(2,1)S(1)} %copy-done.4, bf16[256,2048]{1,0:T(8,128)(2,1)} %fusion.9, bf16[1024,176]{1,0:T(8,128)(2,1)S(1)} %copy.27, bf16[1024,256]{1,0:T(8,128)(2,1)S(1)} %fusion.28), kind=kOutput, calls=%fused_computation | convolution fusion | flops 1819344896 | bytes 6848512 | tf_op jit(solution)/shard_map/dot_general | solution.py:19
  97.5 34.5 %scatter_sum.1 = bf16[64,2048]{1,0:T(8,128)(2,1)} custom-call(bf16[4,2,2,64,2048]{4,3,2,1,0:T(8,128)(2,1)} %bitcast.46, bf16[32,2048]{1,0:T(8,128)(2,1)} %get-tuple-element.10.first), custom_call_target="tpu_custom_call" | custom-call | tf_op jit(solution)/shard_map/scatter_sum/pallas_call | solution.py:481
  132.1 1.7 %copy.29 = bf16[64,2048]{1,0:T(8,128)(2,1)} copy(bf16[64,2048]{1,0:T(8,128)(2,1)} %scatter_sum.1) | data formatting | bytes 524288
  (4 shorter events, 0.1 us)
Async XLA Ops:
  70.7 3.5 %copy-start.1 = (f32[16,8,128]{2,1,0:T(8,128)S(1)}, f32[16,8,128]{2,1,0:T(8,128)}, u32[]{:S(2)}) copy-start(f32[16,8,128]{2,1,0:T(8,128)} %get-tuple-element.8) | copy-start | bytes 196612
  70.7 3.6 %copy-start.5 = (s32[16]{0:T(128)S(1)}, s32[16]{0:T(128)}, u32[]{:S(2)}) copy-start(s32[16]{0:T(128)} %iota_multiply_fusion) | copy-start | bytes 196
  70.7 4.3 %copy-start.2 = (bf16[2048,176]{0,1:T(8,128)(2,1)S(1)}, bf16[2048,176]{0,1:T(8,128)(2,1)}, u32[]{:S(2)}) copy-start(bf16[2048,176]{0,1:T(8,128)(2,1)} %param.40) | copy-start | bytes 2162692
  74.7 4.1 %copy-start = (bf16[4,2,2,64,2048]{4,3,2,1,0:T(8,128)(2,1)S(1)}, bf16[4,2,2,64,2048]{4,3,2,1,0:T(8,128)(2,1)}, u32[]{:S(2)}) copy-start(bf16[4,2,2,64,2048]{4,3,2,1,0:T(8,128)(2,1)} %get-tuple-element.9) | copy-start | bytes 12582916
  74.7 4.1 %copy-start.3 = (bf16[2048,176]{0,1:T(8,128)(2,1)S(1)}, bf16[2048,176]{0,1:T(8,128)(2,1)}, u32[]{:S(2)}) copy-start(bf16[2048,176]{0,1:T(8,128)(2,1)} %param.41) | copy-start | bytes 2162692
  85.7 6.3 %copy-start.4 = (bf16[176,2048]{1,0:T(8,128)(2,1)S(1)}, bf16[176,2048]{1,0:T(8,128)(2,1)}, u32[]{:S(2)}) copy-start(bf16[176,2048]{1,0:T(8,128)(2,1)} %param.42) | copy-start | bytes 2162692
